TPU v7x, 32 devices: a whole 2x2x4 slice. The times are simulated.
32 devices in a mesh: fs: 4 (over z), rep: 4 (over y, x), tp: 2 (over core).
Axes of the slice: x: 2, y: 2, z: 4, core: 2. Of those that a mesh axis runs over, the one named last changes fastest.
Arguments:
- inputs: bfloat16 [4096, 2048], P(('fs', 'rep')), may hold values from -6 to 6
- cot_query: bfloat16 [4096, 2048], P(('fs', 'rep'), 'tp'), may hold values from -0.09375 to 0.09375
- cot_key: bfloat16 [4096, 512], P(('fs', 'rep'), 'tp'), may hold values from -0.09375 to 0.09375
- basis_query: bfloat16 [2048, 512], P('fs'), may hold values from -0.125 to 0.125
- basis_key: bfloat16 [2048, 512], P('fs'), may hold values from -0.125 to 0.125
- weight_query: float32 [2048, 2048], P('fs', 'tp'), may hold values from -0.125 to 0.125
- weight_key: float32 [2048, 512], P('fs', 'tp'), may hold values from -0.125 to 0.125
- moments_query: float32 [2, 512, 2048], P(None, 'fs', 'tp'), may hold values from -8 to 8, as said below
- moments_key: float32 [2, 512, 512], P(None, 'fs', 'tp'), may hold values from -8 to 8, as said below
Outputs:
- step_query: float32 [2048, 2048], P('fs', 'tp')
- step_key: float32 [2048, 512], P('fs', 'tp')
- new_weight_query: float32 [2048, 2048], P('fs', 'tp')
- new_weight_key: float32 [2048, 512], P('fs', 'tp')
- copy_query: bfloat16 [2048, 2048], P(None, 'tp')
- copy_key: bfloat16 [2048, 512], P(None, 'tp')
- new_moments_query: float32 [2, 512, 2048], P(None, 'fs', 'tp')
- new_moments_key: float32 [2, 512, 512], P(None, 'fs', 'tp')
Inputs may be any that keep to these rules, and one draw needn't show every extreme that they name: `moments_query`: entry 1 along the first dimension is positive. `moments_key`: entry 1 along the first dimension is positive.
All inputs are finite; a program needn't handle non-finite values.
Results may differ from a plain program's by a relative error of at most 0.009.
Values may be sent and summed in bfloat16 or wider, within the bound.
A program may use at most 64 MiB of HBM per device.

v0:
```python
import jax
import jax.numpy as jnp
from jax import lax
from jax.sharding import PartitionSpec as P


def plain_contract(left, right):
    return lax.dot_general(
        left, right, (((0,), (0,)), ((), ())), preferred_element_type=jnp.float32
    )


def split_contract(values, cotangent):
    leading = values.astype(jnp.bfloat16)
    remainder = (values - leading.astype(jnp.float32)).astype(jnp.bfloat16)
    return plain_contract(leading, cotangent) + plain_contract(remainder, cotangent)


def moment_update(moments, grad_low):
    first = 0.9 * moments[0] + 0.1 * grad_low
    second = 0.95 * moments[1] + 0.05 * grad_low * grad_low
    normed = first / (jnp.sqrt(second) + 1e-08)
    return (jnp.stack([first, second]), normed)


def on_device(
    inputs,
    cot_query,
    cot_key,
    basis_query,
    basis_key,
    weight_query,
    weight_key,
    moments_query,
    moments_key,
):
    query_cols = cot_query.shape[1]
    whole_query, whole_key = (
        lax.all_gather(basis_query, "fs", axis=0, tiled=True),
        lax.all_gather(basis_key, "fs", axis=0, tiled=True),
    )
    token_query = jnp.dot(inputs, whole_query, preferred_element_type=jnp.float32)
    token_key = jnp.dot(inputs, whole_key, preferred_element_type=jnp.float32)
    low_terms = jnp.concatenate(
        [split_contract(token_query, cot_query), split_contract(token_key, cot_key)], axis=1
    )
    low = lax.psum_scatter(low_terms, "fs", scatter_dimension=0, tiled=True)
    low = lax.psum(low, "rep")
    new_moments_query, normed_query = moment_update(moments_query, low[:, :query_cols])
    new_moments_key, normed_key = moment_update(moments_key, low[:, query_cols:])
    totals = lax.psum(
        (jnp.sum(normed_query * normed_query), jnp.sum(normed_key * normed_key)), ("fs", "tp")
    )
    spread = lax.axis_size("fs") * lax.axis_size("tp")
    scale_query = lax.rsqrt(totals[0] / (normed_query.size * spread) + 1e-06)
    scale_key = lax.rsqrt(totals[1] / (normed_key.size * spread) + 1e-06)
    directions = jnp.concatenate(
        [normed_query.astype(jnp.bfloat16), normed_key.astype(jnp.bfloat16)], axis=1
    )
    piece = lax.all_gather(directions, "fs", axis=0, tiled=True)
    query_term = jnp.dot(basis_query, piece[:, :query_cols], preferred_element_type=jnp.float32)
    key_term = jnp.dot(basis_key, piece[:, query_cols:], preferred_element_type=jnp.float32)
    raw_step = jnp.concatenate([query_term, key_term], axis=1)
    step_query = scale_query * raw_step[:, :query_cols]
    step_key = scale_key * raw_step[:, query_cols:]
    new_weight_query = weight_query - 0.02 * step_query
    new_weight_key = weight_key - 0.02 * step_key
    copy_query, copy_key = (
        lax.all_gather(new_weight_query.astype(jnp.bfloat16), "fs", axis=0, tiled=True),
        lax.all_gather(new_weight_key.astype(jnp.bfloat16), "fs", axis=0, tiled=True),
    )
    return (
        step_query,
        step_key,
        new_weight_query,
        new_weight_key,
        copy_query,
        copy_key,
        new_moments_query,
        new_moments_key,
    )


def solution(mesh):
    in_specs = (
        P(("fs", "rep"), None),
        P(("fs", "rep"), "tp"),
        P(("fs", "rep"), "tp"),
        P("fs", None),
        P("fs", None),
        P("fs", "tp"),
        P("fs", "tp"),
        P(None, "fs", "tp"),
        P(None, "fs", "tp"),
    )
    out_specs = (
        P("fs", "tp"),
        P("fs", "tp"),
        P("fs", "tp"),
        P("fs", "tp"),
        P(None, "tp"),
        P(None, "tp"),
        P(None, "fs", "tp"),
        P(None, "fs", "tp"),
    )
    return jax.shard_map(
        on_device, mesh=mesh, in_specs=in_specs, out_specs=out_specs, check_vma=False
    )
```

profile of v0, /device:TPU:0, one launch (start us, length us, event | category | flops | bytes accessed | tf_op | source)
XLA Modules:
  0.0 373.1 jit_solution(2540141860126746444)
XLA Ops:
  8.7 49.3 %all-gather.8.cloned.1.call-done = bf16[2048,512]{1,0:T(8,128)(2,1)} async-done(((bf16[512,512]{1,0:T(8,128)(2,1)}), bf16[2048,512]{1,0:T(8,128)(2,1)}) %all-gather.8.cloned.1.call-update) | async-done | bytes 2097168 | tf_op jit(solution)/shard_map/all_gather | solution.py:40
  58.0 2.3 fusion.18
  60.8 43.2 %all-gather.6.cloned.1.call-done = bf16[2048,512]{1,0:T(8,128)(2,1)} async-done(((bf16[512,512]{1,0:T(8,128)(2,1)}), bf16[2048,512]{1,0:T(8,128)(2,1)}) %all-gather.6.cloned.1.call-update) | async-done | bytes 2097168 | tf_op jit(solution)/shard_map/all_gather | solution.py:39
  104.0 2.3 fusion.17
  107.3 1.7 pad_maximum_fusion
  109.0 51.2 %reduce-scatter.2.cloned.1.call-done = f32[128,1280]{1,0:T(8,128)} async-done(((f32[512,1280]{1,0:T(8,128)}), f32[128,1280]{1,0:T(8,128)}) %reduce-scatter.2.cloned.1.call-update) | async-done | bytes 655376 | tf_op jit(solution)/shard_map/reduce_scatter | solution.py:47
  160.3 49.2 %all-reduce.3.cloned.1.call-done = f32[128,1280]{1,0:T(8,128)} async-done(((f32[128,1280]{1,0:T(8,128)}), f32[128,1280]{1,0:T(8,128)}) %all-reduce.3.cloned.1.call-update) | async-done | bytes 655376 | tf_op jit(solution)/shard_map/psum | solution.py:48
  209.4 1.6 fusion.13
  211.1 2.9 fusion.11
  214.8 2.2 copy.20
  217.0 17.6 %all-reduce = (f32[]{:T(128)}, f32[]{:T(128)}) all-reduce(f32[]{:T(128)} %get-tuple-element.28, f32[]{:T(128)} %get-tuple-element.32), channel_id=1, replica_groups=mesh['fs'=4,'rep'=4,'tp'=2] {'fs','tp'}, use_global_device_ids=true, to_apply=%region_3.0 | all-reduce | flops 2 | bytes 16 | tf_op jit(solution)/shard_map/psum | solution.py:51
  235.2 12.4 %all-gather.10.cloned.1.call-done = bf16[512,1280]{1,0:T(8,128)(2,1)} async-done(((bf16[128,1280]{1,0:T(8,128)(2,1)}), bf16[512,1280]{1,0:T(8,128)(2,1)}) %all-gather.10.cloned.1.call-update) | async-done | bytes 1310736 | tf_op jit(solution)/shard_map/all_gather | solution.py:60
  247.6 2.7 fusion.15
  250.4 1.8 copy.19
  252.9 4.6 %fusion.16 = (bf16[512,1024]{0,1:T(8,128)(2,1)}, f32[512,1024]{0,1:T(8,128)S(1)}, f32[512,1024]{0,1:T(8,128)}) fusion(f32[512,1024]{0,1:T(8,128)} %copy.19, bf16[512,512]{1,0:T(8,128)(2,1)} %param.12, bf16[512,1280]{1,0:T(8,128)(2,1)} %all-gather.10.cloned.1.call-done, f32[]{:T(128)S(6)} %rsqrt.6), kind=kOutput, calls=%fused_computation.36 | convolution fusion | flops 538968064 | bytes 8912900 | tf_op jit(solution)/shard_map/dot_general | solution.py:61
  258.3 2.3 pad_maximum_fusion.1
  260.6 2.9 copy.21
  263.4 2.0 copy.22
  265.5 1.8 copy.23
  267.3 2.0 copy.24
  269.3 8.3 %all-gather.14.cloned.1.call-done = bf16[2048,256]{0,1:T(8,128)(2,1)} async-done(((bf16[512,256]{0,1:T(8,128)(2,1)}), bf16[2048,256]{0,1:T(8,128)(2,1)}) %all-gather.14.cloned.1.call-update) | async-done | bytes 1048592 | tf_op jit(solution)/shard_map/all_gather | solution.py:70
  277.6 2.3 copy.26
  279.8 80.0 %all-gather.12.cloned.1.call-done = bf16[2048,1024]{0,1:T(8,128)(2,1)} async-done(((bf16[512,1024]{0,1:T(8,128)(2,1)}), bf16[2048,1024]{0,1:T(8,128)(2,1)}) %all-gather.12.cloned.1.call-update) | async-done | bytes 4194320 | tf_op jit(solution)/shard_map/all_gather | solution.py:69
  359.9 6.4 %copy.25 = bf16[2048,1024]{1,0:T(8,128)(2,1)} copy(bf16[2048,1024]{0,1:T(8,128)(2,1)} %all-gather.12.cloned.1.call-done) | data formatting | bytes 8388608
  (32 shorter events, 4.7 us)
Async XLA Ops:
  7.2 50.8 %copy-start = (bf16[256,2048]{1,0:T(8,128)(2,1)S(1)}, bf16[256,2048]{1,0:T(8,128)(2,1)}, u32[]{:S(2)}) copy-start(bf16[256,2048]{1,0:T(8,128)(2,1)} %param.9) | copy-start | bytes 3145732
  7.2 50.8 %all-gather.8.cloned.1.call-start = ((), (), s32[]{:S(2)}) async-start(), calls=%async_computation.2 | async-start | bytes 2621440 | tf_op jit(solution)/shard_map/all_gather | solution.py:40
  7.9 52.4 %copy-start.4 = (bf16[256,256]{1,0:T(8,128)(2,1)S(1)}, bf16[256,256]{1,0:T(8,128)(2,1)}, u32[]{:S(2)}) copy-start(bf16[256,256]{1,0:T(8,128)(2,1)} %param.11) | copy-start | bytes 393220
  7.9 96.1 %all-gather.6.cloned.1.call-start = ((), (), s32[]{:S(2)}) async-start(), calls=%async_computation.1 | async-start | bytes 2621440 | tf_op jit(solution)/shard_map/all_gather | solution.py:39
  8.7 151.5 %reduce-scatter.2.cloned.1.call-start = ((), (), s32[]{:S(2)}) async-start(), calls=%async_computation.3 | async-start | bytes 3276800 | tf_op jit(solution)/shard_map/reduce_scatter | solution.py:47
  60.8 45.5 %copy-start.2 = (bf16[256,1024]{1,0:T(8,128)(2,1)S(1)}, bf16[256,1024]{1,0:T(8,128)(2,1)}, u32[]{:S(2)}) copy-start(bf16[256,1024]{1,0:T(8,128)(2,1)} %param.10) | copy-start | bytes 1572868
  109.0 100.5 %copy-start.5 = (f32[2,128,256]{2,1,0:T(8,128)S(1)}, f32[2,128,256]{2,1,0:T(8,128)}, u32[]{:S(2)}) copy-start(f32[2,128,256]{2,1,0:T(8,128)} %param.17) | copy-start | bytes 786436
  109.0 102.1 %copy-start.3 = (f32[2,128,1024]{2,1,0:T(8,128)S(1)}, f32[2,128,1024]{2,1,0:T(8,128)}, u32[]{:S(2)}) copy-start(f32[2,128,1024]{2,1,0:T(8,128)} %param.16) | copy-start | bytes 3145732
  109.0 100.4 %all-reduce.3.cloned.1.call-start = ((), (), s32[]{:S(2)}) async-start(), calls=%async_computation.4 | async-start | bytes 1310720 | tf_op jit(solution)/shard_map/psum | solution.py:48
  160.2 87.4 %all-gather.10.cloned.1.call-start = ((), (), s32[]{:S(2)}) async-start(), calls=%async_computation.5 | async-start | bytes 1638400 | tf_op jit(solution)/shard_map/all_gather | solution.py:60
  214.7 35.7 %copy-start.1 = (f32[512,1024]{1,0:T(8,128)S(1)}, f32[512,1024]{1,0:T(8,128)}, u32[]{:S(2)}) copy-start(f32[512,1024]{1,0:T(8,128)} %param.14) | copy-start | bytes 6291460
  214.8 62.8 %all-gather.14.cloned.1.call-start = ((), (), s32[]{:S(2)}) async-start(), calls=%async_computation.7 | async-start | bytes 1310720 | tf_op jit(solution)/shard_map/all_gather | solution.py:70
  250.4 109.5 %all-gather.12.cloned.1.call-start = ((), (), s32[]{:S(2)}) async-start(), calls=%async_computation.6 | async-start | bytes 5242880 | tf_op jit(solution)/shard_map/all_gather | solution.py:69
Sparse Core Ops, SparseCore 0:
  9.6 48.3 all-gather.7
  59.5 44.4 all-gather.5
  109.1 51.0 reduce-scatter.1
  163.1 46.3 all-reduce.2
  214.9 32.7 all-gather.9
  250.5 27.0 all-gather.13
  279.7 80.1 all-gather.11
where the time goes:
time: 374 us; the launch traced here: 373 us
  waiting for transfers between devices  295 us (79%)
  local copies, waits for them, and re-layouts  21.4 us (6%)
  blocking collectives  17.6 us (5%)
  between operations  15.6 us (4%)
  matrix products  13.3 us (4%)
  other arithmetic  9.97 us (3%)
    all_gather x1, waiting for transfers between devices, on_device(): lax.all_gather(new_weight_query.astype(jnp.bfloat16), 'fs', axis=0, tiled...  80 us
    reduce_scatter x1, waiting for transfers between devices, on_device(): low = lax.psum_scatter(low_terms, 'fs', scatter_dimension=0, tiled=True)  51.2 us
    all_gather x1, waiting for transfers between devices, on_device(): lax.all_gather(basis_key, 'fs', axis=0, tiled=True)  49.3 us
    psum x1, waiting for transfers between devices, on_device(): low = lax.psum(low, 'rep')  49.2 us
    all_gather x1, waiting for transfers between devices, on_device(): lax.all_gather(basis_query, 'fs', axis=0, tiled=True)  43.2 us
    unnamed x20, local copies, waits for them, and re-layouts  21.4 us
    psum x1, blocking collectives, on_device(): lax.psum((jnp.sum(normed_query * normed_query), jnp.sum(normed_key * norm...  17.6 us
    all_gather x1, waiting for transfers between devices, on_device(): piece = lax.all_gather(directions, 'fs', axis=0, tiled=True)  12.4 us
  transfers between devices with their start and end apart: 7, of which 7 were waited for; matrix products, arithmetic and copies ran while one was open for 7% of the time, Pallas kernels for 0%

commit v1 on v0

v1 whole, which is shorter than its diff:
```python
import functools
import jax
import jax.numpy as jnp
from jax import lax
from jax.experimental import pallas as pl
from jax.experimental.pallas import tpu as pltpu
from jax.sharding import PartitionSpec as P

MESH = pl.DeviceIdType.MESH
LANES = 128


def each(start, stop, body):
    if stop - start <= 4:
        for i in range(start, stop):
            body(i)
    else:
        lax.fori_loop(start, stop, lambda i, carry: (body(i), carry)[1], 0)


def remote(src, dst, send_sem, recv_sem, **device):
    return pltpu.make_async_remote_copy(
        src_ref=src,
        dst_ref=dst,
        send_sem=send_sem,
        recv_sem=recv_sem,
        device_id=device,
        device_id_type=MESH,
    )


def exchange(
    fs,
    rep,
    inputs,
    cot_query,
    cot_key,
    basis,
    wide_query,
    wide_key,
    moments_query,
    moments_key,
    basis_all,
    weight_query_all,
    weight_key_all,
    dir_query,
    dir_key,
    low_query,
    low_key,
    totals,
    factor,
    part_send,
    part_recv,
    slab,
    slab_recv,
    low_all,
    squares,
    pair,
    az_s,
    az_r,
    ap_s,
    ap_r,
    ez_s,
    ez_r,
    ep_s,
    ep_r,
    bp_s,
    bp_r,
    bz_s,
    bz_r,
    lp_s,
    lp_r,
    dz_s,
    dz_r,
    qz_s,
    qz_r,
    pair_s,
    pair_r,
    local,
):
    f, r, c = lax.axis_index("fs"), lax.axis_index("rep"), lax.axis_index("tp")
    height = basis.shape[1]
    part = height // rep
    rank = basis.shape[2]
    rows = rank // fs
    tokens = inputs.shape[0]
    per = part_send.shape[0] // rep
    query_units = cot_query.shape[1] // LANES
    units = query_units + cot_key.shape[1] // LANES

    def ahead(i):
        return lax.rem(f + i, fs)

    def behind(i):
        return lax.rem(f + fs - i, fs)

    def beside(j):
        return lax.rem(r + j, rep)

    def piece(source, owner):
        return pl.ds(pl.multiple_of(source * height + owner * part, part), part)

    own_part = pl.ds(pl.multiple_of(r * part, part), part)
    own_block = pl.ds(pl.multiple_of(f * height, height), height)

    def low_rows(source):
        return pl.ds(pl.multiple_of(source * rows, rows), rows)

    barrier = pltpu.get_barrier_semaphore()

    def greet_fs(i):
        pl.semaphore_signal(barrier, inc=1, device_id={"fs": ahead(i)}, device_id_type=MESH)

    def greet_rep(j):
        pl.semaphore_signal(barrier, inc=1, device_id={"rep": beside(j)}, device_id_type=MESH)

    each(1, fs, greet_fs)
    each(1, rep, greet_rep)
    pl.semaphore_signal(barrier, inc=1, device_id={"tp": 1 - c}, device_id_type=MESH)
    pl.semaphore_wait(barrier, fs + rep - 1)

    def basis_fs(i, source, target):
        return remote(
            basis.at[c, own_part],
            basis_all.at[c, piece(source, r)],
            az_s.at[target],
            az_r.at[source],
            fs=target,
        )

    each(1, fs, lambda i: basis_fs(i, f, ahead(i)).start())

    weights = ((wide_query, weight_query_all), (wide_key, weight_key_all))

    def weight_fs(x, source, target):
        return remote(
            weights[x][0].at[own_part],
            weights[x][1].at[piece(source, r)],
            ez_s.at[x, target],
            ez_r.at[x, source],
            fs=target,
        )

    def weight_rep(x, source, owner, target):
        block = weights[x][1].at[piece(source, owner)]
        return remote(
            block, block, ep_s.at[x, source, target], ep_r.at[x, source, owner], rep=target
        )

    own_copies = [
        pltpu.make_async_copy(basis.at[c], basis_all.at[c, own_block], local.at[0]),
        pltpu.make_async_copy(wide_query, weight_query_all.at[own_block], local.at[1]),
        pltpu.make_async_copy(wide_key, weight_key_all.at[own_block], local.at[2]),
    ]
    for copy in own_copies:
        copy.start()

    def basis_rep(source, owner, target):
        block = basis_all.at[c, piece(source, owner)]
        return remote(block, block, ap_s.at[source, target], ap_r.at[source, owner], rep=target)

    def spread_basis(i):
        source = behind(i)
        basis_fs(i, source, source).wait_recv()
        each(1, rep, lambda j: basis_rep(source, r, beside(j)).start())

    each(1, fs, spread_basis)

    def start_weight(i):
        weight_fs(0, f, ahead(i)).start()
        weight_fs(1, f, ahead(i)).start()

    each(1, fs, start_weight)

    def all_basis(i):
        source = behind(i)
        each(1, rep, lambda j: basis_rep(source, beside(j), beside(j)).wait_recv())

    each(1, fs, all_basis)
    own_copies[0].wait()

    for t in range(0, tokens, LANES):
        value = jnp.dot(
            inputs[t : t + LANES, :], basis_all[c], preferred_element_type=jnp.float32
        )
        factor[c, :, t : t + LANES] = value.T.astype(jnp.bfloat16)
    for u in range(units, per * rep):
        part_send[u] = jnp.zeros(part_send.shape[1:], jnp.bfloat16)
    factor_copy = remote(
        factor.at[c], factor.at[c], pair_s.at[0], pair_r.at[0], tp=1 - c
    )
    factor_back = remote(
        factor.at[1 - c], factor.at[1 - c], pair_s.at[0], pair_r.at[0], tp=1 - c
    )
    factor_copy.start()
    swap = remote(basis_all.at[c], basis_all.at[c], pair_s.at[1], pair_r.at[1], tp=1 - c)
    swap_back = remote(
        basis_all.at[1 - c], basis_all.at[1 - c], pair_s.at[1], pair_r.at[1], tp=1 - c
    )
    factor_back.wait_recv()
    swap.start()

    for x, cot in ((0, cot_query), (1, cot_key)):
        columns = cot.shape[1]
        width = 2 * LANES if columns % (2 * LANES) == 0 else LANES
        for n in range(0, columns, width):
            value = jnp.dot(
                factor[x], cot[:, n : n + width], preferred_element_type=jnp.float32
            ).astype(jnp.bfloat16)
            for k in range(0, width, LANES):
                part_send[x * query_units + (n + k) // LANES] = value[:, k : k + LANES]

    def group(owner):
        return pl.ds(owner * per, per)

    def part_rep(source, target):
        return remote(
            part_send.at[group(target)],
            part_recv.at[source],
            bp_s.at[target],
            bp_r.at[source],
            rep=target,
        )

    each(1, rep, lambda j: part_rep(r, beside(j)).start())
    part_recv[r] = part_send[group(r)]
    each(1, rep, lambda j: part_rep(beside(j), beside(j)).wait_recv())
    for p in range(per):
        value = part_recv[0, p].astype(jnp.float32)
        for q in range(1, rep):
            value = value + part_recv[q, p].astype(jnp.float32)
        slab[p] = value.astype(jnp.bfloat16)

    def slab_fs(source, target):
        return remote(
            slab.at[:, low_rows(target)],
            slab_recv.at[source],
            bz_s.at[target],
            bz_r.at[source],
            fs=target,
        )

    each(1, fs, lambda i: slab_fs(f, ahead(i)).start())

    def spread_weight(i):
        source = behind(i)
        for x in range(2):
            weight_fs(x, source, source).wait_recv()
            each(1, rep, lambda j: weight_rep(x, source, r, beside(j)).start())

    spread_weight(1)
    slab_recv[f] = slab[:, low_rows(f), :]
    each(1, fs, lambda i: slab_fs(behind(i), behind(i)).wait_recv())
    for p in range(per):
        value = slab_recv[0, p].astype(jnp.float32)
        for q in range(1, fs):
            value = value + slab_recv[q, p].astype(jnp.float32)
        low_all[r * per + p] = value.astype(jnp.bfloat16)

    def low_rep(owner, target):
        block = low_all.at[group(owner)]
        return remote(block, block, lp_s.at[target], lp_r.at[owner], rep=target)

    each(1, rep, lambda j: low_rep(r, beside(j)).start())
    each(1, rep, lambda j: low_rep(beside(j), beside(j)).wait_recv())

    for x, moments, direction, low_out in (
        (0, moments_query, dir_query, low_query),
        (1, moments_key, dir_key, low_key),
    ):
        total = jnp.zeros((8, LANES), jnp.float32)
        for n in range(0, moments.shape[2], LANES):
            span = slice(n, n + LANES)
            low = low_all[x * query_units + n // LANES].astype(jnp.float32)
            low_out[:, span] = low
            first = 0.9 * moments[0, :, span] + 0.1 * low
            second = 0.95 * moments[1, :, span] + 0.05 * low * low
            normed = first / (jnp.sqrt(second) + 1e-08)
            direction[low_rows(f), span] = normed.astype(jnp.bfloat16)
            total = total + jnp.sum((normed * normed).reshape(rows // 8, 8, LANES), axis=0)
        squares[f, x] = total

    directions = (dir_query, dir_key)

    def direction_fs(x, source, target):
        block = directions[x].at[low_rows(source)]
        return remote(block, block, dz_s.at[x, target], dz_r.at[x, source], fs=target)

    def squares_fs(source, target):
        block = squares.at[source]
        return remote(block, block, qz_s.at[target], qz_r.at[source], fs=target)

    def start_direction(i):
        squares_fs(f, ahead(i)).start()
        direction_fs(0, f, ahead(i)).start()
        direction_fs(1, f, ahead(i)).start()

    each(1, fs, start_direction)
    each(2, fs, spread_weight)

    each(1, fs, lambda i: squares_fs(behind(i), behind(i)).wait_recv())
    total = squares[0]
    for q in range(1, fs):
        total = total + squares[q]
    pair[c] = total
    total_copy = remote(pair.at[c], pair.at[c], pair_s.at[2], pair_r.at[2], tp=1 - c)
    total_back = remote(pair.at[1 - c], pair.at[1 - c], pair_s.at[2], pair_r.at[2], tp=1 - c)
    total_copy.start()
    total_back.wait_recv()
    totals[...] = pair[0] + pair[1]

    def end_fs(i):
        source, target = behind(i), ahead(i)
        for x in range(2):
            direction_fs(x, source, source).wait_recv()
            each(1, rep, lambda j: weight_rep(x, source, beside(j), beside(j)).wait_recv())
            each(1, rep, lambda j: weight_rep(x, source, r, beside(j)).wait_send())
            weight_fs(x, f, target).wait_send()
            direction_fs(x, f, target).wait_send()
        each(1, rep, lambda j: basis_rep(source, r, beside(j)).wait_send())
        basis_fs(i, f, target).wait_send()
        slab_fs(f, target).wait_send()
        squares_fs(f, target).wait_send()

    def end_rep(j):
        part_rep(r, beside(j)).wait_send()
        low_rep(r, beside(j)).wait_send()

    each(1, fs, end_fs)
    each(1, rep, end_rep)
    swap_back.wait_recv()
    factor_copy.wait_send()
    swap.wait_send()
    total_copy.wait_send()
    own_copies[1].wait()
    own_copies[2].wait()


def on_device(
    inputs,
    cot_query,
    cot_key,
    basis_query,
    basis_key,
    weight_query,
    weight_key,
    moments_query,
    moments_key,
):
    fs, rep, tp = lax.axis_size("fs"), lax.axis_size("rep"), lax.axis_size("tp")
    assert tp == 2
    height, rank = basis_query.shape
    rows = rank // fs
    tokens = inputs.shape[0]
    query_cols, key_cols = cot_query.shape[1], cot_key.shape[1]
    per = -(-((query_cols + key_cols) // LANES) // rep)
    basis = jnp.stack([basis_query, basis_key])
    vmem = pl.BlockSpec(memory_space=pltpu.VMEM)
    hbm = pl.BlockSpec(memory_space=pl.ANY)
    bf16, f32 = jnp.bfloat16, jnp.float32
    dma = pltpu.SemaphoreType.DMA
    shape = jax.ShapeDtypeStruct
    (
        basis_all,
        weight_query_all,
        weight_key_all,
        dir_query,
        dir_key,
        low_query,
        low_key,
        totals,
    ) = pl.pallas_call(
        functools.partial(exchange, fs, rep),
        out_shape=(
            shape((2, height * fs, rank), bf16),
            shape((height * fs, query_cols), bf16),
            shape((height * fs, key_cols), bf16),
            shape((rank, query_cols), bf16),
            shape((rank, key_cols), bf16),
            shape((rows, query_cols), f32),
            shape((rows, key_cols), f32),
            shape((2, 8, LANES), f32),
        ),
        in_specs=[vmem] * 8,
        out_specs=(vmem, hbm, hbm, vmem, vmem, vmem, vmem, vmem),
        scratch_shapes=[
            pltpu.VMEM((2, rank, tokens), bf16),
            pltpu.VMEM((per * rep, rank, LANES), bf16),
            pltpu.VMEM((rep, per, rank, LANES), bf16),
            pltpu.VMEM((per, rank, LANES), bf16),
            pltpu.VMEM((fs, per, rows, LANES), bf16),
            pltpu.VMEM((per * rep, rows, LANES), bf16),
            pltpu.VMEM((fs, 2, 8, LANES), f32),
            pltpu.VMEM((2, 2, 8, LANES), f32),
            dma((fs,)),
            dma((fs,)),
            dma((fs, rep)),
            dma((fs, rep)),
            dma((2, fs)),
            dma((2, fs)),
            dma((2, fs, rep)),
            dma((2, fs, rep)),
            dma((rep,)),
            dma((rep,)),
            dma((fs,)),
            dma((fs,)),
            dma((rep,)),
            dma((rep,)),
            dma((2, fs)),
            dma((2, fs)),
            dma((fs,)),
            dma((fs,)),
            dma((3,)),
            dma((3,)),
            dma((3,)),
        ],
        compiler_params=pltpu.CompilerParams(
            collective_id=0, has_side_effects=True, vmem_limit_bytes=48 * 1024 * 1024
        ),
    )(
        inputs,
        cot_query,
        cot_key,
        basis,
        weight_query.astype(bf16),
        weight_key.astype(bf16),
        moments_query,
        moments_key,
    )

    def finish(x, total, own_basis, direction, weight, weight_all, moments, low):
        scale = lax.rsqrt(jnp.sum(total) / (low.size * fs * tp) + 1e-06)
        step = scale * jnp.dot(own_basis, direction, preferred_element_type=f32)
        new_weight = weight - 0.02 * step
        whole = scale * jnp.dot(basis_all[x], direction, preferred_element_type=f32)
        copy = (weight_all.astype(f32) - 0.02 * whole).astype(bf16)
        first = 0.9 * moments[0] + 0.1 * low
        second = 0.95 * moments[1] + 0.05 * low * low
        return step, new_weight, copy, jnp.stack([first, second])

    query = finish(
        0, totals[0], basis_query, dir_query, weight_query, weight_query_all, moments_query, low_query
    )
    key = finish(1, totals[1], basis_key, dir_key, weight_key, weight_key_all, moments_key, low_key)
    return tuple(value for both in zip(query, key) for value in both)


def solution(mesh):
    in_specs = (
        P(("fs", "rep"), None),
        P(("fs", "rep"), "tp"),
        P(("fs", "rep"), "tp"),
        P("fs", None),
        P("fs", None),
        P("fs", "tp"),
        P("fs", "tp"),
        P(None, "fs", "tp"),
        P(None, "fs", "tp"),
    )
    out_specs = (
        P("fs", "tp"),
        P("fs", "tp"),
        P("fs", "tp"),
        P("fs", "tp"),
        P(None, "tp"),
        P(None, "tp"),
        P(None, "fs", "tp"),
        P(None, "fs", "tp"),
    )
    return jax.shard_map(
        on_device, mesh=mesh, in_specs=in_specs, out_specs=out_specs, check_vma=False
    )
```

time: 374 us -> 145 us (0.39)
  waiting for transfers between devices: 295 us -> 0 us
  Pallas kernels: 0 us -> 107 us
  blocking collectives: 17.6 us -> 0 us
  between operations: 15.6 us -> 2.11 us
  local copies, waits for them, and re-layouts: 21.4 us -> 11.5 us
    all_gather x5 -> x0, waiting for transfers between devices: 193 us -> none  [the longest x1 80 us: on_device(): lax.all_gather(new_weight_query.astype(jnp.bfloat16), 'fs', axis=0, tiled...]
    pallas_call x0 -> x1, Pallas kernels: none -> 107 us  [on_device(): pl.pallas_call(functools.partial(exchange, fs, rep), out_shape=(shape((2,...]
    reduce_scatter x1 -> x0, waiting for transfers between devices: 51.2 us -> none  [on_device(): low = lax.psum_scatter(low_terms, 'fs', scatter_dimension=0, tiled=True)]
    psum x1 -> x0, waiting for transfers between devices: 49.2 us -> none  [on_device(): low = lax.psum(low, 'rep')]
    psum x1 -> x0, blocking collectives: 17.6 us -> none  [on_device(): lax.psum((jnp.sum(normed_query * normed_query), jnp.sum(normed_key * norm...]
    unnamed x20 -> x26, local copies, waits for them, and re-layouts: 21.4 us -> 11.5 us
    dot_general x8 -> x4, matrix products: 13.3 us -> 16.7 us  [the longest x2 10.8 us: finish(): whole = scale * jnp.dot(basis_all[x], direction, preferred_element_type=f32)]
    another operation x4 -> x5, other arithmetic: 7.53 us -> 4.24 us  [the longest x4 3.18 us: finish(): return (step, new_weight, copy, jnp.stack([first, second]))]
  transfers between devices with their start and end apart: 7 -> 0, of which waited for: 7 -> 0; matrix products, arithmetic and copies ran while one was open for 7% -> 0% of each run, Pallas kernels for 0% -> 0%
where the time goes in v1:
time: 145 us
  Pallas kernels  107 us (74%)
  matrix products  16.7 us (12%)
  local copies, waits for them, and re-layouts  11.5 us (8%)
  other arithmetic  7.71 us (5%)
  between operations  2.11 us (1%)
    pallas_call x1, Pallas kernels, on_device(): pl.pallas_call(functools.partial(exchange, fs, rep), out_shape=(shape((2,...  107 us
    unnamed x26, local copies, waits for them, and re-layouts  11.5 us
    dot_general x2, matrix products, finish(): whole = scale * jnp.dot(basis_all[x], direction, preferred_element_type=f32)  10.8 us
    dot_general x2, matrix products, finish(): step = scale * jnp.dot(own_basis, direction, preferred_element_type=f32)  5.92 us
    another operation x4, other arithmetic, finish(): return (step, new_weight, copy, jnp.stack([first, second]))  3.18 us

profile of v1, /device:TPU:0, one launch (start us, length us, event | category | flops | bytes accessed | tf_op | source)
XLA Modules:
  0.0 144.8 jit_solution(2158524505292242044)
XLA Ops:
  0.6 0.0 copy-start.8
  0.6 0.0 copy-start.7
  0.7 2.8 %convert_element_type.18.wide_query = bf16[512,1024]{1,0:T(8,128)(2,1)} convert(f32[512,1024]{1,0:T(8,128)} %param.14) | non-fusion elementwise | flops 524288 | bytes 3145728 | tf_op jit(solution)/shard_map/convert_element_type | solution.py:425
  3.5 1.1 pad_maximum_fusion.basis
  4.6 0.5 copy-done
  5.1 0.0 copy-done.1
  5.2 0.2 copy-done.2
  5.3 0.0 copy-done.3
  5.3 106.8 %shard_map.152 = (bf16[2,2048,512]{2,1,0:T(8,128)(2,1)}, bf16[2048,1024]{1,0:T(8,128)(2,1)}, bf16[2048,256]{1,0:T(8,128)(2,1)S(1)}, bf16[512,1024]{1,0:T(8,128)(...) custom-call(bf16[256,2048]{1,0:T(8,128)(2,1)S(1)} %copy-done, ...), custom_call_target="tpu_custom_call" | custom-call | tf_op jit(solution)/shard_map/pallas_call | solution.py:372
  112.2 0.6 slice_reduce_fusion
  113.4 3.3 %fusion.2 = bf16[2048,256]{1,0:T(8,128)(2,1)} fusion(bf16[512,256]{1,0:T(8,128)(2,1)S(1)} %get-tuple-element.18, bf16[2,2048,512]{2,1,0:T(8,128)(2,1)} %get-tuple-element.20, bf16[2048,256]{1,0:T(8,128)(2,1)S(1)} %get-tuple-element.21, f32[]{:T(128)S(6)} %rsqrt.7), kind=kOutput, calls=%fused_computation.4 | convolution fusion | flops 539492352 | bytes 4456452 | tf_op jit(solution)/shard_map/dot_general | solution.py:435
  117.4 0.0 copy-start.6
  117.4 7.5 %subtract_convert_fusion = bf16[2048,1024]{1,0:T(8,128)(2,1)} fusion(bf16[2048,1024]{1,0:T(8,128)(2,1)} %get-tuple-element.19, bf16[512,1024]{1,0:T(8,128)(2,1)S(1)} %get-tuple-element.17, f32[]{:T(128)S(6)} %rsqrt.6, bf16[2,2048,512]{2,1,0:T(8,128)(2,1)} %get-tuple-element.20), kind=kOutput, calls=%fused_computation | convolution fusion | flops 2157969408 | bytes 11534340 | tf_op jit(solution)/shard_map/dot_general | solution.py:435
  124.9 1.0 copy.18
  125.9 1.6 %multiply_subtract_fusion.1 = (f32[512,256]{0,1:T(8,128)S(1)}, f32[512,256]{0,1:T(8,128)S(1)}) fusion(f32[512,256]{0,1:T(8,128)} %copy.18, bf16[512,256]{1,0:T(8,128)(2,1)S(1)} %get-tuple-element.18, bf16[512,512]{1,0:T(8,128)(2,1)} %param.13, f32[]{:T(128)S(6)} %rsqrt.7), kind=kOutput, calls=%fused_computation.20 | convolution fusion | flops 134610944 | bytes 2359300 | tf_op jit(solution)/shard_map/dot_general | solution.py:433
  127.5 1.0 copy.20
  128.5 1.0 copy.22
  129.5 2.9 %copy.17 = f32[512,1024]{0,1:T(8,128)} copy(f32[512,1024]{1,0:T(8,128)} %param.14) | data formatting | bytes 4194304 | tf_op args[5]
  132.4 4.4 %multiply_subtract_fusion = (f32[512,1024]{0,1:T(8,128)}, f32[512,1024]{0,1:T(8,128)}) fusion(f32[512,1024]{0,1:T(8,128)} %copy.17, bf16[512,1024]{1,0:T(8,128)(2,1)S(1)} %get-tuple-element.17, bf16[512,512]{1,0:T(8,128)(2,1)S(1)} %copy-done.9, f32[]{:T(128)S(6)} %rsqrt.6), kind=kOutput, calls=%fused_computation.9 | convolution fusion | flops 538443776 | bytes 7864324 | tf_op jit(solution)/shard_map/dot_general | solution.py:433
  136.8 3.0 %copy.19 = f32[512,1024]{1,0:T(8,128)} copy(f32[512,1024]{0,1:T(8,128)} %get-tuple-element.39) | data formatting | bytes 4194304
  139.8 1.8 %copy.21 = f32[512,1024]{1,0:T(8,128)} copy(f32[512,1024]{0,1:T(8,128)S(1)} %copy-done.4) | data formatting | bytes 4194304
  141.6 1.4 fusion.10
  143.0 1.0 pad_maximum_fusion.1
  144.1 0.7 pad_maximum_fusion.2
  (15 shorter events, 0.1 us)
Async XLA Ops:
  0.6 2.9 %copy-start.8 = (bf16[512,512]{1,0:T(8,128)(2,1)S(1)}, bf16[512,512]{1,0:T(8,128)(2,1)}, u32[]{:S(2)}) copy-start(bf16[512,512]{1,0:T(8,128)(2,1)} %param.12) | copy-start | bytes 1572868
  0.6 2.9 %copy-start.7 = (bf16[512,512]{1,0:T(8,128)(2,1)S(1)}, bf16[512,512]{1,0:T(8,128)(2,1)}, u32[]{:S(2)}) copy-start(bf16[512,512]{1,0:T(8,128)(2,1)} %param.13) | copy-start | bytes 1572868
  0.7 3.9 %copy-start.5 = (f32[512,256]{1,0:T(8,128)S(1)}, f32[512,256]{1,0:T(8,128)}, u32[]{:S(2)}) copy-start(f32[512,256]{1,0:T(8,128)} %param.15) | copy-start | bytes 1572868
  3.5 1.6 %copy-start = (bf16[256,2048]{1,0:T(8,128)(2,1)S(1)}, bf16[256,2048]{1,0:T(8,128)(2,1)}, u32[]{:S(2)}) copy-start(bf16[256,2048]{1,0:T(8,128)(2,1)} %inputs.1) | copy-start | bytes 3145732
  3.5 1.6 %copy-start.1 = (f32[2,128,256]{2,1,0:T(8,128)S(1)}, f32[2,128,256]{2,1,0:T(8,128)}, u32[]{:S(2)}) copy-start(f32[2,128,256]{2,1,0:T(8,128)} %moments_key.1) | copy-start | bytes 786436
  3.5 1.8 %copy-start.2 = (bf16[256,1024]{1,0:T(8,128)(2,1)S(1)}, bf16[256,1024]{1,0:T(8,128)(2,1)}, u32[]{:S(2)}) copy-start(bf16[256,1024]{1,0:T(8,128)(2,1)} %cot_query.1) | copy-start | bytes 1572868
  3.5 1.8 %copy-start.3 = (bf16[256,256]{1,0:T(8,128)(2,1)S(1)}, bf16[256,256]{1,0:T(8,128)(2,1)}, u32[]{:S(2)}) copy-start(bf16[256,256]{1,0:T(8,128)(2,1)} %cot_key.1) | copy-start | bytes 393220
  117.4 7.5 %copy-start.6 = (f32[512,256]{1,0:T(8,128)S(1)}, f32[512,256]{1,0:T(8,128)}, u32[]{:S(2)}) copy-start(f32[512,256]{1,0:T(8,128)} %param.15) | copy-start | bytes 1572868
  129.5 2.9 %copy-start.9 = (bf16[512,512]{1,0:T(8,128)(2,1)S(1)}, bf16[512,512]{1,0:T(8,128)(2,1)}, u32[]{:S(2)}) copy-start(bf16[512,512]{1,0:T(8,128)(2,1)} %param.12) | copy-start | bytes 1572868
  136.8 3.0 %copy-start.4 = (f32[512,1024]{0,1:T(8,128)S(1)}, f32[512,1024]{0,1:T(8,128)}, u32[]{:S(2)}) copy-start(f32[512,1024]{0,1:T(8,128)} %get-tuple-element.38) | copy-start | bytes 6291460

commit v2 on v1

--- a/solution.py
+++ b/solution.py
@@ -35,9 +35,10 @@
     inputs,
     cot_query,
     cot_key,
-    basis,
-    wide_query,
-    wide_key,
+    basis_query,
+    basis_key,
+    full_query,
+    full_key,
     moments_query,
     moments_key,
     basis_all,
@@ -48,6 +49,10 @@
     low_query,
     low_key,
     totals,
+    loaded_query,
+    loaded_key,
+    wide_query,
+    wide_key,
     factor,
     part_send,
     part_recv,
@@ -70,7 +75,8 @@
     bz_r,
     lp_s,
     lp_r,
-    dz_s,
+    dr_s,
+    dl_s,
     dz_r,
     qz_s,
     qz_r,
@@ -79,9 +85,9 @@
     local,
 ):
     f, r, c = lax.axis_index("fs"), lax.axis_index("rep"), lax.axis_index("tp")
-    height = basis.shape[1]
+    height = basis_query.shape[0]
     part = height // rep
-    rank = basis.shape[2]
+    rank = basis_query.shape[1]
     rows = rank // fs
     tokens = inputs.shape[0]
     per = part_send.shape[0] // rep
@@ -97,6 +103,16 @@
     def beside(j):
         return lax.rem(r + j, rep)
 
+    near = r + 1 - 2 * lax.rem(r, 2)
+    far = r + 2 - 4 * (r // 2)
+    across = 3 - r
+    owners = (r, r, near, far)
+    targets = (near, far, far, near)
+    senders = (near, far, across, across)
+
+    def span_of(slot, width):
+        return (pl.ds(0, width), pl.ds(0, width), pl.ds(0, width // 2), pl.ds(width // 2, width // 2))[slot]
+
     def piece(source, owner):
         return pl.ds(pl.multiple_of(source * height + owner * part, part), part)
 
@@ -106,6 +122,12 @@
     def low_rows(source):
         return pl.ds(pl.multiple_of(source * rows, rows), rows)
 
+    loads = [
+        pltpu.make_async_copy(full_query, loaded_query, local.at[3]),
+        pltpu.make_async_copy(full_key, loaded_key, local.at[4]),
+    ]
+    for load in loads:
+        load.start()
     barrier = pltpu.get_barrier_semaphore()
 
     def greet_fs(i):
@@ -119,18 +141,32 @@
     pl.semaphore_signal(barrier, inc=1, device_id={"tp": 1 - c}, device_id_type=MESH)
     pl.semaphore_wait(barrier, fs + rep - 1)
 
-    def basis_fs(i, source, target):
+    bases = (basis_query, basis_key)
+    weights = ((wide_query, weight_query_all), (wide_key, weight_key_all))
+
+    def basis_fs(x, source, target):
         return remote(
-            basis.at[c, own_part],
+            bases[x].at[own_part],
             basis_all.at[c, piece(source, r)],
             az_s.at[target],
             az_r.at[source],
             fs=target,
         )
 
-    each(1, fs, lambda i: basis_fs(i, f, ahead(i)).start())
-
-    weights = ((wide_query, weight_query_all), (wide_key, weight_key_all))
+    for x in range(2):
+
+        @pl.when(c == x)
+        def start_basis():
+            each(1, fs, lambda i: basis_fs(x, f, ahead(i)).start())
+            pltpu.make_async_copy(bases[x], basis_all.at[c, own_block], local.at[0]).start()
+
+    own_basis = pltpu.make_async_copy(basis_query, basis_all.at[c, own_block], local.at[0])
+
+    def basis_hop(source, slot, owner):
+        block = basis_all.at[c, piece(source, owner), span_of(slot, rank)]
+        return remote(
+            block, block, ap_s.at[source, slot], ap_r.at[source, slot], rep=targets[slot]
+        )
 
     def weight_fs(x, source, target):
         return remote(
@@ -141,43 +177,51 @@
             fs=target,
         )
 
-    def weight_rep(x, source, owner, target):
-        block = weights[x][1].at[piece(source, owner)]
+    def weight_hop(x, source, slot, owner):
+        block = weights[x][1].at[piece(source, owner), span_of(slot, weights[x][1].shape[1])]
         return remote(
-            block, block, ep_s.at[x, source, target], ep_r.at[x, source, owner], rep=target
-        )
+            block, block, ep_s.at[x, source, slot], ep_r.at[x, source, slot], rep=targets[slot]
+        )
+
+    for load in loads:
+        load.wait()
+    wide_query[...] = loaded_query[...].astype(jnp.bfloat16)
+    wide_key[...] = loaded_key[...].astype(jnp.bfloat16)
+
+    def spread_basis(i):
+        source = behind(i)
+        basis_fs(0, source, source).wait_recv()
+        for slot in (0, 1):
+            basis_hop(source, slot, owners[slot]).start()
+
+    each(1, fs, spread_basis)
 
     own_copies = [
-        pltpu.make_async_copy(basis.at[c], basis_all.at[c, own_block], local.at[0]),
         pltpu.make_async_copy(wide_query, weight_query_all.at[own_block], local.at[1]),
         pltpu.make_async_copy(wide_key, weight_key_all.at[own_block], local.at[2]),
     ]
     for copy in own_copies:
         copy.start()
 
-    def basis_rep(source, owner, target):
-        block = basis_all.at[c, piece(source, owner)]
-        return remote(block, block, ap_s.at[source, target], ap_r.at[source, owner], rep=target)
-
-    def spread_basis(i):
-        source = behind(i)
-        basis_fs(i, source, source).wait_recv()
-        each(1, rep, lambda j: basis_rep(source, r, beside(j)).start())
-
-    each(1, fs, spread_basis)
-
     def start_weight(i):
         weight_fs(0, f, ahead(i)).start()
         weight_fs(1, f, ahead(i)).start()
 
     each(1, fs, start_weight)
 
+    def relay_basis(i):
+        source = behind(i)
+        for slot in (0, 1):
+            basis_hop(source, slot, senders[slot]).wait_recv()
+            basis_hop(source, slot + 2, owners[slot + 2]).start()
+
     def all_basis(i):
-        source = behind(i)
-        each(1, rep, lambda j: basis_rep(source, beside(j), beside(j)).wait_recv())
-
+        for slot in (2, 3):
+            basis_hop(behind(i), slot, senders[slot]).wait_recv()
+
+    each(1, fs, relay_basis)
     each(1, fs, all_basis)
-    own_copies[0].wait()
+    own_basis.wait()
 
     for t in range(0, tokens, LANES):
         value = jnp.dot(
@@ -246,7 +290,15 @@
         source = behind(i)
         for x in range(2):
             weight_fs(x, source, source).wait_recv()
-            each(1, rep, lambda j: weight_rep(x, source, r, beside(j)).start())
+            for slot in (0, 1):
+                weight_hop(x, source, slot, owners[slot]).start()
+
+    def relay_weight(i):
+        source = behind(i)
+        for slot in (0, 1):
+            for x in range(2):
+                weight_hop(x, source, slot, senders[slot]).wait_recv()
+                weight_hop(x, source, slot + 2, owners[slot + 2]).start()
 
     spread_weight(1)
     slab_recv[f] = slab[:, low_rows(f), :]
@@ -282,21 +334,58 @@
 
     directions = (dir_query, dir_key)
 
-    def direction_fs(x, source, target):
+    right, left = ahead(1), behind(1)
+
+    def move_right(x, source):
         block = directions[x].at[low_rows(source)]
-        return remote(block, block, dz_s.at[x, target], dz_r.at[x, source], fs=target)
+        return remote(block, block, dr_s.at[x, source], dz_r.at[x, source], fs=right)
+
+    def move_left(x, source):
+        block = directions[x].at[low_rows(source)]
+        return remote(block, block, dl_s.at[x, source], dz_r.at[x, source], fs=left)
 
     def squares_fs(source, target):
         block = squares.at[source]
         return remote(block, block, qz_s.at[target], qz_r.at[source], fs=target)
 
-    def start_direction(i):
-        squares_fs(f, ahead(i)).start()
-        direction_fs(0, f, ahead(i)).start()
-        direction_fs(1, f, ahead(i)).start()
-
-    each(1, fs, start_direction)
+    each(1, fs, lambda i: squares_fs(f, ahead(i)).start())
+
+    @pl.when(f + 1 < fs)
+    def start_right():
+        for x in range(2):
+            move_right(x, f).start()
+
+    @pl.when(f > 0)
+    def start_left():
+        for x in range(2):
+            move_left(x, f).start()
+
     each(2, fs, spread_weight)
+
+    def relay_direction(k):
+        @pl.when(f - k >= 0)
+        def from_left():
+            for x in range(2):
+                move_right(x, f - k).wait_recv()
+
+                @pl.when(f + 1 < fs)
+                def onward():
+                    move_right(x, f - k).start()
+
+        @pl.when(f + k < fs)
+        def from_right():
+            for x in range(2):
+                move_left(x, f + k).wait_recv()
+
+                @pl.when(f > 0)
+                def onward():
+                    move_left(x, f + k).start()
+
+    def relay_both(k):
+        relay_weight(k)
+        relay_direction(k)
+
+    each(1, fs, relay_both)
 
     each(1, fs, lambda i: squares_fs(behind(i), behind(i)).wait_recv())
     total = squares[0]
@@ -312,28 +401,98 @@
     def end_fs(i):
         source, target = behind(i), ahead(i)
         for x in range(2):
-            direction_fs(x, source, source).wait_recv()
-            each(1, rep, lambda j: weight_rep(x, source, beside(j), beside(j)).wait_recv())
-            each(1, rep, lambda j: weight_rep(x, source, r, beside(j)).wait_send())
+            for slot in (2, 3):
+                weight_hop(x, source, slot, senders[slot]).wait_recv()
+            for slot in range(4):
+                weight_hop(x, source, slot, owners[slot]).wait_send()
             weight_fs(x, f, target).wait_send()
-            direction_fs(x, f, target).wait_send()
-        each(1, rep, lambda j: basis_rep(source, r, beside(j)).wait_send())
-        basis_fs(i, f, target).wait_send()
+        for slot in range(4):
+            basis_hop(source, slot, owners[slot]).wait_send()
+        basis_fs(0, f, target).wait_send()
         slab_fs(f, target).wait_send()
         squares_fs(f, target).wait_send()
+
+    def end_direction(k):
+        @pl.when((f - k >= 0) & (f + 1 < fs))
+        def end_right():
+            for x in range(2):
+                move_right(x, f - k).wait_send()
+
+        @pl.when((f + k < fs) & (f > 0))
+        def end_left():
+            for x in range(2):
+                move_left(x, f + k).wait_send()
 
     def end_rep(j):
         part_rep(r, beside(j)).wait_send()
         low_rep(r, beside(j)).wait_send()
 
     each(1, fs, end_fs)
+    each(0, fs, end_direction)
     each(1, rep, end_rep)
     swap_back.wait_recv()
     factor_copy.wait_send()
     swap.wait_send()
     total_copy.wait_send()
-    own_copies[1].wait()
-    own_copies[2].wait()
+    for copy in own_copies:
+        copy.wait()
+
+
+def apply(
+    count_query,
+    count_key,
+    totals,
+    dir_query,
+    dir_key,
+    low_query,
+    low_key,
+    moments_query,
+    moments_key,
+    basis_all,
+    weight_query_all,
+    weight_key_all,
+    basis_query,
+    basis_key,
+    weight_query,
+    weight_key,
+    step_query,
+    step_key,
+    new_weight_query,
+    new_weight_key,
+    copy_query,
+    copy_key,
+    new_moments_query,
+    new_moments_key,
+):
+    parts = (
+        (count_query, dir_query, weight_query_all, basis_query, weight_query),
+        (count_key, dir_key, weight_key_all, basis_key, weight_key),
+    )
+    outs = (
+        (step_query, new_weight_query, copy_query),
+        (step_key, new_weight_key, copy_key),
+    )
+    for x in range(2):
+        count, direction, weight_all, basis, weight = parts[x]
+        step_out, new_weight_out, copy_out = outs[x]
+        scale = lax.rsqrt(jnp.sum(totals[x], keepdims=True) / count + 1e-06)
+        step = scale * jnp.dot(basis[...], direction[...], preferred_element_type=jnp.float32)
+        step_out[...] = step
+        new_weight_out[...] = weight[...] - 0.02 * step
+        whole = scale * jnp.dot(
+            basis_all[x], direction[...], preferred_element_type=jnp.float32
+        )
+        copy_out[...] = (weight_all[...].astype(jnp.float32) - 0.02 * whole).astype(jnp.bfloat16)
+
+    @pl.when(pl.program_id(0) == 0)
+    def moments_once():
+        for moments, low_ref, out in (
+            (moments_query, low_query, new_moments_query),
+            (moments_key, low_key, new_moments_key),
+        ):
+            low = low_ref[...]
+            out[0] = 0.9 * moments[0] + 0.1 * low
+            out[1] = 0.95 * moments[1] + 0.05 * low * low
 
 
 def on_device(
@@ -348,13 +507,12 @@
     moments_key,
 ):
     fs, rep, tp = lax.axis_size("fs"), lax.axis_size("rep"), lax.axis_size("tp")
-    assert tp == 2
+    assert tp == 2 and rep == 4
     height, rank = basis_query.shape
     rows = rank // fs
     tokens = inputs.shape[0]
     query_cols, key_cols = cot_query.shape[1], cot_key.shape[1]
     per = -(-((query_cols + key_cols) // LANES) // rep)
-    basis = jnp.stack([basis_query, basis_key])
     vmem = pl.BlockSpec(memory_space=pltpu.VMEM)
     hbm = pl.BlockSpec(memory_space=pl.ANY)
     bf16, f32 = jnp.bfloat16, jnp.float32
@@ -381,9 +539,13 @@
             shape((rows, key_cols), f32),
             shape((2, 8, LANES), f32),
         ),
-        in_specs=[vmem] * 8,
+        in_specs=[vmem] * 5 + [hbm, hbm, vmem, vmem],
         out_specs=(vmem, hbm, hbm, vmem, vmem, vmem, vmem, vmem),
         scratch_shapes=[
+            pltpu.VMEM((height, query_cols), f32),
+            pltpu.VMEM((height, key_cols), f32),
+            pltpu.VMEM((height, query_cols), bf16),
+            pltpu.VMEM((height, key_cols), bf16),
             pltpu.VMEM((2, rank, tokens), bf16),
             pltpu.VMEM((per * rep, rank, LANES), bf16),
             pltpu.VMEM((rep, per, rank, LANES), bf16),
@@ -408,41 +570,97 @@
             dma((rep,)),
             dma((2, fs)),
             dma((2, fs)),
+            dma((2, fs)),
             dma((fs,)),
             dma((fs,)),
             dma((3,)),
             dma((3,)),
-            dma((3,)),
+            dma((5,)),
         ],
         compiler_params=pltpu.CompilerParams(
-            collective_id=0, has_side_effects=True, vmem_limit_bytes=48 * 1024 * 1024
+            collective_id=0, has_side_effects=True, vmem_limit_bytes=32 * 1024 * 1024
         ),
     )(
         inputs,
         cot_query,
         cot_key,
-        basis,
-        weight_query.astype(bf16),
-        weight_key.astype(bf16),
+        basis_query,
+        basis_key,
+        weight_query,
+        weight_key,
         moments_query,
         moments_key,
     )
 
-    def finish(x, total, own_basis, direction, weight, weight_all, moments, low):
-        scale = lax.rsqrt(jnp.sum(total) / (low.size * fs * tp) + 1e-06)
-        step = scale * jnp.dot(own_basis, direction, preferred_element_type=f32)
-        new_weight = weight - 0.02 * step
-        whole = scale * jnp.dot(basis_all[x], direction, preferred_element_type=f32)
-        copy = (weight_all.astype(f32) - 0.02 * whole).astype(bf16)
-        first = 0.9 * moments[0] + 0.1 * low
-        second = 0.95 * moments[1] + 0.05 * low * low
-        return step, new_weight, copy, jnp.stack([first, second])
-
-    query = finish(
-        0, totals[0], basis_query, dir_query, weight_query, weight_query_all, moments_query, low_query
-    )
-    key = finish(1, totals[1], basis_key, dir_key, weight_key, weight_key_all, moments_key, low_key)
-    return tuple(value for both in zip(query, key) for value in both)
+    steps = min(8, height // 16)
+    tall, short = height * fs // steps, height // steps
+
+    def fixed(*dims):
+        return pl.BlockSpec(dims, lambda i: (0,) * len(dims))
+
+    def banded(*dims):
+        return pl.BlockSpec(dims, lambda i: (i, 0))
+
+    owned = tuple(
+        shape((height, columns), f32) for columns in (query_cols, key_cols, query_cols, key_cols)
+    )
+    owned_specs = tuple(
+        banded(short, columns) for columns in (query_cols, key_cols, query_cols, key_cols)
+    )
+    return pl.pallas_call(
+        functools.partial(
+            apply, float(rank * query_cols * tp), float(rank * key_cols * tp)
+        ),
+        grid=(steps,),
+        out_shape=owned
+        + (
+            shape((height * fs, query_cols), bf16),
+            shape((height * fs, key_cols), bf16),
+            shape((2, rows, query_cols), f32),
+            shape((2, rows, key_cols), f32),
+        ),
+        in_specs=[
+            fixed(2, 8, LANES),
+            fixed(rank, query_cols),
+            fixed(rank, key_cols),
+            fixed(rows, query_cols),
+            fixed(rows, key_cols),
+            fixed(2, rows, query_cols),
+            fixed(2, rows, key_cols),
+            pl.BlockSpec((2, tall, rank), lambda i: (0, i, 0)),
+            banded(tall, query_cols),
+            banded(tall, key_cols),
+            banded(short, rank),
+            banded(short, rank),
+            banded(short, query_cols),
+            banded(short, key_cols),
+        ],
+        out_specs=owned_specs
+        + (
+            banded(tall, query_cols),
+            banded(tall, key_cols),
+            fixed(2, rows, query_cols),
+            fixed(2, rows, key_cols),
+        ),
+        compiler_params=pltpu.CompilerParams(
+            dimension_semantics=("arbitrary",), vmem_limit_bytes=32 * 1024 * 1024
+        ),
+    )(
+        totals,
+        dir_query,
+        dir_key,
+        low_query,
+        low_key,
+        moments_query,
+        moments_key,
+        basis_all,
+        weight_query_all,
+        weight_key_all,
+        basis_query,
+        basis_key,
+        weight_query,
+        weight_key,
+    )
 
 
 def solution(mesh):

time: 145 us -> 112 us (0.77)
  matrix products: 16.7 us -> 0 us
  other arithmetic: 7.71 us -> 0 us
  Pallas kernels: 107 us -> 99.8 us
    dot_general x4 -> x0, matrix products: 16.7 us -> none  [the longest x2 10.8 us: finish(): whole = scale * jnp.dot(basis_all[x], direction, preferred_element_type=f32)]
    pallas_call x1, Pallas kernels: 107 us -> 91.1 us  [on_device(): pl.pallas_call(functools.partial(exchange, fs, rep), out_shape=(shape((2,...]
    pallas_call x0 -> x1, Pallas kernels: none -> 8.72 us  [on_device(): pl.pallas_call(functools.partial(apply, float(rank * query_cols * tp), fl...]
    another operation x5 -> x0, other arithmetic: 4.24 us -> none  [the longest x4 3.18 us: finish(): return (step, new_weight, copy, jnp.stack([first, second]))]
    convert_element_type x2 -> x0, other arithmetic: 2.87 us -> none  [the longest x1 2.84 us: on_device(): weight_query.astype(bf16)]
    unnamed x26 -> x22, local copies, waits for them, and re-layouts: 11.5 us -> 10.1 us
where the time goes in v2:
time: 112 us; the launch traced here: 111 us
  Pallas kernels  99.8 us (89%)
  local copies, waits for them, and re-layouts  10.1 us (9%)
    pallas_call x1, Pallas kernels, on_device(): pl.pallas_call(functools.partial(exchange, fs, rep), out_shape=(shape((2,...  91.1 us
    unnamed x22, local copies, waits for them, and re-layouts  10.1 us
    pallas_call x1, Pallas kernels, on_device(): pl.pallas_call(functools.partial(apply, float(rank * query_cols * tp), fl...  8.72 us

profile of v2, /device:TPU:0, one launch (start us, length us, event | category | flops | bytes accessed | tf_op | source)
XLA Modules:
  0.0 110.5 jit_solution(17288940207248052242)
XLA Ops:
  0.6 0.0 copy-start
  0.6 1.6 %copy-done = f32[512,1024]{1,0:T(8,128)S(1)} copy-done((f32[512,1024]{1,0:T(8,128)S(1)}, f32[512,1024]{1,0:T(8,128)}, u32[]{:S(2)}) %copy-start) | copy-done | bytes 2097176
  2.2 0.0 copy-start.2
  2.2 1.2 %copy-done.2 = f32[2,128,1024]{2,1,0:T(8,128)S(1)} copy-done((f32[2,128,1024]{2,1,0:T(8,128)S(1)}, f32[2,128,1024]{2,1,0:T(8,128)}, u32[]{:S(2)}) %copy-start.2) | copy-done | bytes 1048600
  3.5 0.0 copy-start.3
  3.5 1.0 copy-done.3
  4.5 0.0 copy-start.4
  4.5 1.0 copy-done.4
  5.5 0.0 copy-start.5
  5.5 1.0 copy-done.5
  6.6 0.0 copy-start.7
  6.6 0.9 copy-done.7
  7.5 0.0 copy-start.8
  7.5 1.2 %copy-done.8 = bf16[256,2048]{1,0:T(8,128)(2,1)S(1)} copy-done((bf16[256,2048]{1,0:T(8,128)(2,1)S(1)}, bf16[256,2048]{1,0:T(8,128)(2,1)}, u32[]{:S(2)}) %copy-start.8) | copy-done | bytes 1048600
  8.8 0.0 copy-start.9
  8.8 1.0 copy-done.9
  9.8 0.0 copy-start.10
  9.8 0.9 copy-done.10
  10.7 0.0 copy-start.1
  10.7 0.0 copy-start.6
  10.7 91.1 %shard_map.152 = (bf16[2,2048,512]{2,1,0:T(8,128)(2,1)S(1)}, bf16[2048,1024]{1,0:T(8,128)(2,1)S(1)}, bf16[2048,256]{1,0:T(8,128)(2,1)S(1)}, bf16[512,1024]{1,0:T...) custom-call(bf16[256,2048]{1,0:T(8,128)(2,1)S(1)} %copy-done.8, ...), custom_call_target="tpu_custom_call" | custom-call | tf_op jit(solution)/shard_map/pallas_call | solution.py:530
  101.8 0.0 copy-done.1
  101.8 0.0 copy-done.6
  101.8 8.7 %shard_map.153 = (f32[512,1024]{1,0:T(8,128)}, f32[512,256]{1,0:T(8,128)}, f32[512,1024]{1,0:T(8,128)}, f32[512,256]{1,0:T(8,128)}, bf16[2048,1024]{1,0:T(8,128)...) custom-call(f32[2,8,128]{2,1,0:T(8,128)S(1)} %get-tuple-element.16.totals, ...), custom_call_target="tpu_custom_call" | custom-call | tf_op jit(solution)/shard_map/pallas_call | solution.py:610
Async XLA Ops:
  0.6 1.6 %copy-start = (f32[512,1024]{1,0:T(8,128)S(1)}, f32[512,1024]{1,0:T(8,128)}, u32[]{:S(2)}) copy-start(f32[512,1024]{1,0:T(8,128)} %weight_query.1) | copy-start | bytes 6291460
  2.2 1.2 %copy-start.2 = (f32[2,128,1024]{2,1,0:T(8,128)S(1)}, f32[2,128,1024]{2,1,0:T(8,128)}, u32[]{:S(2)}) copy-start(f32[2,128,1024]{2,1,0:T(8,128)} %moments_query.3) | copy-start | bytes 3145732
  3.5 1.0 copy-start.3
  4.5 1.0 copy-start.4
  5.5 1.0 copy-start.5
  6.6 0.9 copy-start.7
  7.5 1.2 %copy-start.8 = (bf16[256,2048]{1,0:T(8,128)(2,1)S(1)}, bf16[256,2048]{1,0:T(8,128)(2,1)}, u32[]{:S(2)}) copy-start(bf16[256,2048]{1,0:T(8,128)(2,1)} %inputs.1) | copy-start | bytes 3145732
  8.8 1.0 copy-start.9
  9.8 0.9 copy-start.10
  10.7 91.1 %copy-start.1 = (f32[512,1024]{1,0:T(8,128)S(1)}, f32[512,1024]{1,0:T(8,128)}, u32[]{:S(2)}) copy-start(f32[512,1024]{1,0:T(8,128)} %weight_query.1) | copy-start | bytes 6291460
  10.7 91.1 %copy-start.6 = (f32[512,256]{1,0:T(8,128)S(1)}, f32[512,256]{1,0:T(8,128)}, u32[]{:S(2)}) copy-start(f32[512,256]{1,0:T(8,128)} %weight_key.1) | copy-start | bytes 1572868

commit v3 on v2

--- a/solution.py
+++ b/solution.py
@@ -32,15 +32,15 @@
 def exchange(
     fs,
     rep,
-    inputs,
-    cot_query,
-    cot_key,
+    inputs_far,
+    cot_query_far,
+    cot_key_far,
     basis_query,
     basis_key,
     full_query,
     full_key,
-    moments_query,
-    moments_key,
+    moments_query_far,
+    moments_key_far,
     basis_all,
     weight_query_all,
     weight_key_all,
@@ -49,6 +49,11 @@
     low_query,
     low_key,
     totals,
+    inputs,
+    cot_query,
+    cot_key,
+    moments_query,
+    moments_key,
     loaded_query,
     loaded_key,
     wide_query,
@@ -123,11 +128,19 @@
         return pl.ds(pl.multiple_of(source * rows, rows), rows)
 
     loads = [
-        pltpu.make_async_copy(full_query, loaded_query, local.at[3]),
-        pltpu.make_async_copy(full_key, loaded_key, local.at[4]),
+        pltpu.make_async_copy(source, target, local.at[3 + n])
+        for n, (source, target) in enumerate(
+            (
+                (full_query, loaded_query),
+                (full_key, loaded_key),
+                (inputs_far, inputs),
+                (cot_query_far, cot_query),
+                (cot_key_far, cot_key),
+                (moments_query_far, moments_query),
+                (moments_key_far, moments_key),
+            )
+        )
     ]
-    for load in loads:
-        load.start()
     barrier = pltpu.get_barrier_semaphore()
 
     def greet_fs(i):
@@ -160,6 +173,8 @@
             each(1, fs, lambda i: basis_fs(x, f, ahead(i)).start())
             pltpu.make_async_copy(bases[x], basis_all.at[c, own_block], local.at[0]).start()
 
+    for load in loads:
+        load.start()
     own_basis = pltpu.make_async_copy(basis_query, basis_all.at[c, own_block], local.at[0])
 
     def basis_hop(source, slot, owner):
@@ -183,7 +198,7 @@
             block, block, ep_s.at[x, source, slot], ep_r.at[x, source, slot], rep=targets[slot]
         )
 
-    for load in loads:
+    for load in loads[:2]:
         load.wait()
     wide_query[...] = loaded_query[...].astype(jnp.bfloat16)
     wide_key[...] = loaded_key[...].astype(jnp.bfloat16)
@@ -222,6 +237,8 @@
     each(1, fs, relay_basis)
     each(1, fs, all_basis)
     own_basis.wait()
+    for load in loads[2:]:
+        load.wait()
 
     for t in range(0, tokens, LANES):
         value = jnp.dot(
@@ -539,9 +556,14 @@
             shape((rows, key_cols), f32),
             shape((2, 8, LANES), f32),
         ),
-        in_specs=[vmem] * 5 + [hbm, hbm, vmem, vmem],
+        in_specs=[pl.BlockSpec(memory_space=pltpu.HBM)] * 9,
         out_specs=(vmem, hbm, hbm, vmem, vmem, vmem, vmem, vmem),
         scratch_shapes=[
+            pltpu.VMEM((tokens, inputs.shape[1]), bf16),
+            pltpu.VMEM((tokens, query_cols), bf16),
+            pltpu.VMEM((tokens, key_cols), bf16),
+            pltpu.VMEM((2, rows, query_cols), f32),
+            pltpu.VMEM((2, rows, key_cols), f32),
             pltpu.VMEM((height, query_cols), f32),
             pltpu.VMEM((height, key_cols), f32),
             pltpu.VMEM((height, query_cols), bf16),
@@ -575,21 +597,26 @@
             dma((fs,)),
             dma((3,)),
             dma((3,)),
-            dma((5,)),
+            dma((10,)),
         ],
         compiler_params=pltpu.CompilerParams(
             collective_id=0, has_side_effects=True, vmem_limit_bytes=32 * 1024 * 1024
         ),
     )(
-        inputs,
-        cot_query,
-        cot_key,
-        basis_query,
-        basis_key,
-        weight_query,
-        weight_key,
-        moments_query,
-        moments_key,
+        *(
+            pltpu.with_memory_space_constraint(operand, pltpu.HBM)
+            for operand in (
+                inputs,
+                cot_query,
+                cot_key,
+                basis_query,
+                basis_key,
+                weight_query,
+                weight_key,
+                moments_query,
+                moments_key,
+            )
+        )
     )
 
     steps = min(8, height // 16)

time: 112 us -> 101 us (0.902)
  local copies, waits for them, and re-layouts: 10.1 us -> 0.03 us
    unnamed x22 -> x12, local copies, waits for them, and re-layouts: 10.1 us -> 0.03 us
where the time goes in v3:
time: 101 us
  Pallas kernels  99.8 us (99%)
    pallas_call x1, Pallas kernels, on_device(): pl.pallas_call(functools.partial(exchange, fs, rep), out_shape=(shape((2,...  91.1 us
    pallas_call x1, Pallas kernels, on_device(): pl.pallas_call(functools.partial(apply, float(rank * query_cols * tp), fl...  8.65 us

profile of v3, /device:TPU:0, one launch (start us, length us, event | category | flops | bytes accessed | tf_op | source)
XLA Modules:
  0.0 100.5 jit_solution(11985207674569250137)
XLA Ops:
  0.6 0.0 copy-start.5
  0.6 0.0 copy-start.1
  0.7 0.0 copy-start.4
  0.7 0.0 copy-start
  0.7 0.0 copy-start.3
  0.7 0.0 copy-start.2
  0.7 91.1 %shard_map.152 = (bf16[2,2048,512]{2,1,0:T(8,128)(2,1)S(1)}, bf16[2048,1024]{1,0:T(8,128)(2,1)S(1)}, bf16[2048,256]{1,0:T(8,128)(2,1)S(1)}, bf16[512,1024]{1,0:T...) custom-call(bf16[256,2048]{1,0:T(8,128)(2,1)} %inputs_far.1, ...), custom_call_target="tpu_custom_call" | custom-call | tf_op jit(solution)/shard_map/pallas_call | solution.py:547
  91.8 0.0 copy-done.5
  91.8 0.0 copy-done.1
  91.8 0.0 copy-done.4
  91.8 0.0 copy-done
  91.9 0.0 copy-done.3
  91.9 0.0 copy-done.2
  91.9 8.7 %shard_map.153 = (f32[512,1024]{1,0:T(8,128)}, f32[512,256]{1,0:T(8,128)}, f32[512,1024]{1,0:T(8,128)}, f32[512,256]{1,0:T(8,128)}, bf16[2048,1024]{1,0:T(8,128)...) custom-call(f32[2,8,128]{2,1,0:T(8,128)S(1)} %get-tuple-element.16.totals, ...), custom_call_target="tpu_custom_call" | custom-call | tf_op jit(solution)/shard_map/pallas_call | solution.py:637
Async XLA Ops:
  0.6 91.2 %copy-start.5 = (f32[2,128,256]{2,1,0:T(8,128)S(1)}, f32[2,128,256]{2,1,0:T(8,128)}, u32[]{:S(2)}) copy-start(f32[2,128,256]{2,1,0:T(8,128)} %moments_key.1) | copy-start | bytes 786436
  0.6 91.2 %copy-start.1 = (f32[2,128,1024]{2,1,0:T(8,128)S(1)}, f32[2,128,1024]{2,1,0:T(8,128)}, u32[]{:S(2)}) copy-start(f32[2,128,1024]{2,1,0:T(8,128)} %moments_query.1) | copy-start | bytes 3145732
  0.7 91.2 %copy-start.4 = (f32[512,256]{1,0:T(8,128)S(1)}, f32[512,256]{1,0:T(8,128)}, u32[]{:S(2)}) copy-start(f32[512,256]{1,0:T(8,128)} %weight_key.1) | copy-start | bytes 1572868
  0.7 91.2 %copy-start = (f32[512,1024]{1,0:T(8,128)S(1)}, f32[512,1024]{1,0:T(8,128)}, u32[]{:S(2)}) copy-start(f32[512,1024]{1,0:T(8,128)} %weight_query.1) | copy-start | bytes 6291460
  0.7 91.2 %copy-start.3 = (bf16[512,512]{1,0:T(8,128)(2,1)S(1)}, bf16[512,512]{1,0:T(8,128)(2,1)}, u32[]{:S(2)}) copy-start(bf16[512,512]{1,0:T(8,128)(2,1)} %basis_key.3) | copy-start | bytes 1572868
  0.7 91.2 %copy-start.2 = (bf16[512,512]{1,0:T(8,128)(2,1)S(1)}, bf16[512,512]{1,0:T(8,128)(2,1)}, u32[]{:S(2)}) copy-start(bf16[512,512]{1,0:T(8,128)(2,1)} %basis_query.3) | copy-start | bytes 1572868
